TPU v7x, 256 devices: a whole 4x4x8 slice. The times are simulated.
256 devices in a mesh: kv: 32 (over z, x), tp: 8 (over y, core).
Axes of the slice: x: 4, y: 4, z: 8, core: 2. Of those that a mesh axis runs over, the one named last changes fastest.
Arguments:
- tokens: bfloat16 [16, 2048], P(None, ('kv', 'tp')), may hold values from -60 to 60, as said below
- w_query: bfloat16 [2048, 1024], P('kv', 'tp'), may hold values from -0.125 to 0.125
- w_key: bfloat16 [2048, 1024], P('kv', 'tp'), may hold values from -0.125 to 0.125
- w_value: bfloat16 [2048, 1024], P('kv', 'tp'), may hold values from -0.125 to 0.125
- w_forget: bfloat16 [2048, 8], replicated, may hold values from -0.125 to 0.125
- w_out: bfloat16 [1024, 2048], P('tp', 'kv'), may hold values from -1 to 1, as said below
- mix_gain: float32 [2048], P(('kv', 'tp')), may hold values from 0.1 to 1.9
- mix_bias: float32 [2048], P(('kv', 'tp')), may hold values from -3 to 3
- ffn_gain: float32 [2048], P(('kv', 'tp')), may hold values from 0.1 to 1.9
- ffn_bias: float32 [2048], P(('kv', 'tp')), may hold values from -3 to 3
- w_up: bfloat16 [2048, 8192], P('kv', 'tp'), may hold values from -0.125 to 0.125
- down_weight: bfloat16 [8192, 2048], P('tp', 'kv'), may hold values from -0.5 to 0.5, as said below
- cache_keys: bfloat16 [16, 8, 16384, 128], P(None, 'tp', 'kv'), may hold values from -200 to 200, as said below
- cache_values: bfloat16 [16, 8, 16384, 128], P(None, 'tp', 'kv'), may hold values from -24 to 24
- cum_gates: float32 [16, 8, 16384], P(None, 'tp', 'kv'), as said below
Outputs:
- result: bfloat16 [16, 2048], P(None, ('kv', 'tp'))
Inputs may be any that keep to these rules, and one draw needn't show every extreme that they name: `tokens`: real-valued rows. `cache_keys`: real-valued keys. `cum_gates`: sums of log gates. `w_out`: real-valued weights. `down_weight`: real-valued weights.
All inputs are finite; a program needn't handle non-finite values.
Results may differ from a plain program's by a relative error of at most 0.0075.
Values may be sent and summed in bfloat16 or wider, within the bound.
A program may use at most 64 MiB of HBM per device.

v0:
```python
import jax
import jax.numpy as jnp
from jax import lax
from jax.sharding import Mesh
from jax.sharding import PartitionSpec as P

D = 2048
HEAD_DIM = 128
TP = ("tp_0", "tp_1")
KV = ("kv_0", "kv_1")
KV_TP = ("kv_0", "kv_1", "tp_0", "tp_1")


residual_scale = 1.4142135623730951
norm_eps = 1e-05


def from_everyone(shard, axis):
    length = lax.axis_size(axis)
    return lax.all_to_all(
        jnp.broadcast_to(shard[None], (length, *shard.shape)), axis, 0, 0, tiled=True
    )


def joined_along(tiles, dim):
    lengths = list(tiles.shape[1:])
    lengths[dim] *= tiles.shape[0]
    return jnp.moveaxis(tiles, 0, dim).reshape(lengths)


def gather_directly(shard, axis, dim):
    tiles = from_everyone(shard, axis)
    return joined_along(tiles, dim)


def of_everyone(shard, axis):
    return from_everyone(shard, axis).sum(axis=0)


def together(arrays, axis):
    flat, at, done = (jnp.concatenate([a.reshape(-1) for a in arrays]), 0, [])
    so_far = of_everyone(flat, axis)
    for a in arrays:
        done.append(so_far[at : at + a.size].reshape(a.shape))
        at += a.size
    return tuple(done)


def collected_together(shard, axis):
    leaves = jax.tree.leaves(shard)
    turns = sorted(range(len(leaves)), key=lambda k: -leaves[k].size)
    width = (1, *leaves[turns[0]].shape)[-1]
    lines = [
        jnp.pad(leaves[k].reshape(-1), (0, -leaves[k].size % width)).reshape(-1, width)
        for k in turns
    ]
    both, at, found = (from_everyone(jnp.concatenate(lines), axis), 0, {})
    for k, line in zip(turns, lines):
        share = both[:, at : at + len(line)].reshape(len(both), -1)
        found[k] = share[:, : leaves[k].size].reshape(-1, *leaves[k].shape)
        at += len(line)
    numbers = iter(range(len(leaves)))
    return jax.tree.map(lambda _: found[next(numbers)], shard)


def folded_in_pairs(pieces, combine):
    while len(jax.tree.leaves(pieces)[0]) > 1:
        pieces = jax.vmap(combine)(
            *(jax.tree.map(lambda part: part[side::2], pieces) for side in (0, 1))
        )
    return jax.tree.map(lambda part: part[0], pieces)


def joined_all(shard, axis, combine):
    pieces = collected_together(shard, axis)
    return folded_in_pairs(pieces, combine)


def split_up(shard, dim, length):
    before, after = (shard.shape[:dim], shard.shape[dim + 1 :])
    return jnp.moveaxis(shard.reshape(*before, length, -1, *after), dim, 0)


def sent_and_summed(shard, axis, dim):
    length = lax.axis_size(axis)
    tiles = lax.all_to_all(split_up(shard, dim, length), axis, 0, 0, tiled=True)
    return jnp.sum(tiles, axis=0)


def over_axes(shard, axes):
    far, near = axes
    return of_everyone(of_everyone(shard, near), far)


def together_2(arrays, axis):
    ends = [0]
    for a in arrays:
        ends.append(ends[-1] + a.size)
    so_far = over_axes(jnp.concatenate([a.ravel() for a in arrays]), axis)
    return tuple((so_far[b:e].reshape(a.shape) for a, b, e in zip(arrays, ends, ends[1:])))


def padded_to(lines, length):
    spare = -len(lines) % length
    return jnp.pad(lines, [(0, spare)] + [(0, 0)] * (lines.ndim - 1))


def nested_sum(shard, axes):
    lines = shard.reshape(-1)
    padded = padded_to(lines, lax.axis_size(axes))
    whole = gather_directly(sent_and_summed(padded, axes, 0), axes, 0)
    return lax.slice_in_dim(whole, 0, len(lines)).reshape(shard.shape)


def combine_parts(earlier, later):
    peak_one, total_one, accum_one = earlier
    peak_two, total_two, accum_two = later
    peak_both = jnp.maximum(peak_one, peak_two)
    factor_one = jnp.exp(peak_one - peak_both)
    factor_two = jnp.exp(peak_two - peak_both)
    total_both = factor_one * total_one + factor_two * total_two
    accum_both = factor_one[..., None] * accum_one + factor_two[..., None] * accum_two
    return (peak_both, total_both, accum_both)


def apply_norm(residual_sum, row_sums, row_squares, gain, bias):
    row_mean = (row_sums / D)[:, None]
    row_var = (row_squares / D)[:, None] - row_mean * row_mean
    return (residual_sum - row_mean) * lax.rsqrt(row_var + norm_eps) * gain + bias


def shards(
    tokens,
    w_query,
    w_key,
    w_value,
    w_forget,
    w_out,
    mix_gain,
    mix_bias,
    ffn_gain,
    ffn_bias,
    w_up,
    down_weight,
    cache_keys,
    cache_values,
    cum_gates,
):
    batch_entries = tokens.shape[0]
    heads_here = cache_keys.shape[1]
    rows_here = w_query.shape[0]
    local_columns = gather_directly(tokens, TP, 1)
    gate_rows = lax.dynamic_slice_in_dim(w_forget, lax.axis_index(KV) * rows_here, rows_here, 0)
    gate_columns = lax.dynamic_slice_in_dim(
        gate_rows, lax.axis_index(TP) * heads_here, heads_here, 1
    )
    partials = (
        jnp.dot(local_columns, w_query, preferred_element_type=jnp.float32),
        jnp.dot(local_columns, w_key, preferred_element_type=jnp.float32),
        jnp.dot(local_columns, w_value, preferred_element_type=jnp.float32),
        jnp.dot(local_columns, gate_columns, preferred_element_type=jnp.float32),
    )
    query_sum, summed_key_total, value_sum, gate_sum = together(
        (partials[0], partials[1], partials[2], partials[3]), KV
    )
    query_heads = query_sum.astype(jnp.bfloat16).reshape(batch_entries, heads_here, HEAD_DIM)
    key_heads = summed_key_total.astype(jnp.bfloat16).reshape(batch_entries, heads_here, HEAD_DIM)
    value_heads = value_sum.astype(jnp.bfloat16).reshape(batch_entries, heads_here, HEAD_DIM)
    log_forget = jax.nn.log_sigmoid(gate_sum)
    score_scale = HEAD_DIM ** (-0.5)
    scores = (
        jnp.einsum("bhd,bhpd->bhp", query_heads, cache_keys, preferred_element_type=jnp.float32)
        * score_scale
    )
    scores = scores + cum_gates + log_forget[:, :, None]
    peak_score = jnp.max(scores, axis=-1)
    weights = jnp.exp(scores - peak_score[..., None])
    weight_total = jnp.sum(weights, axis=-1)
    weighted = jnp.einsum(
        "bhp,bhpd->bhd",
        weights.astype(jnp.bfloat16),
        cache_values,
        preferred_element_type=jnp.float32,
    )
    merged = joined_all((peak_score, weight_total, weighted), KV, combine_parts)
    own_score = (
        jnp.sum(query_heads.astype(jnp.float32) * key_heads.astype(jnp.float32), axis=-1)
        * score_scale
    )
    own_part = (own_score, jnp.ones_like(own_score), value_heads.astype(jnp.float32))
    peak_all, denom, numer = combine_parts(merged, own_part)
    attended = (
        (numer / denom[..., None])
        .astype(jnp.bfloat16)
        .reshape(batch_entries, heads_here * HEAD_DIM)
    )
    head_terms = jnp.dot(attended, w_out, preferred_element_type=jnp.float32)
    mixed = residual_scale * tokens.astype(jnp.float32) + sent_and_summed(head_terms, TP, 1)
    mix_sums, mix_squares = together_2(
        (jnp.sum(mixed, axis=-1), jnp.sum(mixed * mixed, axis=-1)),
        (("kv_0", "kv_1"), ("tp_0", "tp_1")),
    )
    normed = apply_norm(mixed, mix_sums, mix_squares, mix_gain, mix_bias).astype(jnp.bfloat16)
    normed_kv = gather_directly(normed, TP, 1)
    up_terms = jnp.dot(normed_kv, w_up, preferred_element_type=jnp.float32)
    up_proj = nested_sum(up_terms, KV)
    hidden = jnp.square(jax.nn.relu(up_proj)).astype(jnp.bfloat16)
    down_terms = jnp.dot(hidden, down_weight, preferred_element_type=jnp.float32)
    outer = residual_scale * normed.astype(jnp.float32) + sent_and_summed(down_terms, TP, 1)
    result_accumulations, out_squares = together_2(
        (jnp.sum(outer, axis=-1), jnp.sum(outer * outer, axis=-1)),
        (("kv_0", "kv_1"), ("tp_0", "tp_1")),
    )
    return apply_norm(outer, result_accumulations, out_squares, ffn_gain, ffn_bias).astype(
        jnp.bfloat16
    )


def solution(mesh):
    finer = Mesh(mesh.devices.reshape(8, 4, 4, 2), ("kv_0", "kv_1", "tp_0", "tp_1"))
    return jax.shard_map(
        shards,
        mesh=finer,
        in_specs=(
            P(None, KV_TP),
            P(KV, TP),
            P(KV, TP),
            P(KV, TP),
            P(),
            P(TP, KV),
            P(KV_TP),
            P(KV_TP),
            P(KV_TP),
            P(KV_TP),
            P(KV, TP),
            P(TP, KV),
            P(None, TP, KV, None),
            P(None, TP, KV, None),
            P(None, TP, KV),
        ),
        out_specs=P(None, KV_TP),
        check_vma=False,
    )
```

profile of v0, /device:TPU:1, one launch (start us, length us, event | category | flops | bytes accessed | tf_op | source)
XLA Modules:
  0.0 168.1 jit_solution(6840069394268481238)
XLA Ops:
  0.0 0.0 copy-start
  0.0 1.4 broadcast_in_dim.18
  1.4 6.4 %all-to-all-start = ((bf16[8,16,8]{1,2,0:T(8,128)(2,1)}), bf16[8,16,8]{1,2,0:T(8,128)(2,1)S(1)}, u32[]{:S(2)}, u32[]{:S(2)}) async-start(bf16[8,16,8]{1,2,0:T(8,128)(2,1)} %broadcast_in_dim.18), calls=%async_computation | async-start | bytes 32768 | tf_op jit(solution)/shard_map/all_to_all | solution.py:20
  7.9 4.7 %all-to-all-done = bf16[8,16,8]{1,2,0:T(8,128)(2,1)S(1)} async-done(((bf16[8,16,8]{1,2,0:T(8,128)(2,1)}), bf16[8,16,8]{1,2,0:T(8,128)(2,1)S(1)}, u32[]{:S(2)}, u32[]{:S(2)}) %all-to-all-start) | async-done | bytes 2080 | tf_op jit(solution)/shard_map/all_to_all | solution.py:20
  12.5 0.9 convolution_bitcast_fusion.2
  13.4 0.9 convolution_bitcast_fusion.3
  14.3 0.9 convolution_bitcast_fusion.4
  15.2 0.9 convolution_bitcast_fusion.5
  16.1 0.4 broadcast_in_dim.19
  16.5 0.0 copy-start.3
  16.5 31.7 %all_to_all.71 = f32[32,1,6160]{2,1,0:T(1,128)S(1)} all-to-all(f32[32,1,6160]{2,1,0:T(1,128)S(1)} %broadcast_in_dim.19), channel_id=1, replica_groups=mesh['kv_0'=8,'kv_1'=4,'tp_0'=4,'tp_1'=2] {'kv_0','kv_1'}, dimensions={0} | all-to-all | bytes 1576960 | tf_op jit(solution)/shard_map/all_to_all | solution.py:20
  48.2 0.5 reduce_sum.126
  48.7 0.0 copy-start.9
  48.7 0.0 copy-done
  48.7 0.6 fusion.2
  49.4 0.0 copy-done.3
  49.4 0.3 fusion.48
  49.7 0.3 fusion.45
  50.0 0.3 copy-done.9
  50.3 0.4 fusion
  50.7 0.0 copy-start.6
  50.7 0.0 copy-start.2
  50.7 0.8 broadcast_in_dim.20
  51.5 6.0 %all-to-all-start.2 = ((f32[32,18,128]{2,1,0:T(8,128)}), f32[32,18,128]{2,1,0:T(8,128)S(1)}, u32[]{:S(2)}, u32[]{:S(2)}) async-start(f32[32,18,128]{2,1,0:T(8,128)} %broadcast_in_dim.20), calls=%async_computation.2 | async-start | bytes 786432 | tf_op jit(solution)/shard_map/all_to_all | solution.py:20
  57.5 0.1 bitcast_reduce_fusion
  57.6 12.4 %all-to-all-done.2 = f32[32,18,128]{2,1,0:T(8,128)S(1)} async-done(((f32[32,18,128]{2,1,0:T(8,128)}), f32[32,18,128]{2,1,0:T(8,128)S(1)}, u32[]{:S(2)}, u32[]{:S(2)}) %all-to-all-start.2) | async-done | bytes 294944 | tf_op jit(solution)/shard_map/all_to_all | solution.py:20
  70.6 0.1 multiply_add_fusion
  70.8 0.1 multiply_add_fusion.1
  70.9 0.1 multiply_add_fusion.2
  71.0 0.1 multiply_add_fusion.3
  71.0 0.0 copy-done.10
  71.0 0.2 fusion.50
  71.2 0.1 reshape.436
  71.3 10.6 %all_to_all.72 = f32[8,1,128]{2,1,0:T(1,128)S(1)} all-to-all(f32[8,1,128]{2,1,0:T(1,128)S(1)} %reshape.436), channel_id=1, replica_groups=mesh['kv_0'=8,'kv_1'=4,'tp_0'=4,'tp_1'=2] {'tp_0','tp_1'}, dimensions={0} | all-to-all | bytes 8192 | tf_op jit(solution)/shard_map/all_to_all | solution.py:86
  81.9 0.5 broadcast.174
  82.5 0.7 reduce.12
  83.1 0.1 reshape.437
  83.2 0.0 copy-done.4
  83.2 0.1 pad_maximum_fusion.2
  83.3 7.6 %all_to_all.73 = f32[8,1,32]{2,1,0:T(1,128)S(1)} all-to-all(f32[8,1,32]{2,1,0:T(1,128)S(1)} %broadcast_in_dim.21), channel_id=1, replica_groups=mesh['kv_0'=8,'kv_1'=4,'tp_0'=4,'tp_1'=2] {'tp_0','tp_1'}, dimensions={0} | all-to-all | bytes 2048 | tf_op jit(solution)/shard_map/all_to_all | solution.py:20
  91.0 12.5 %all_to_all.74 = f32[32,1,32]{2,1,0:T(1,128)S(1)} all-to-all(f32[32,1,32]{2,1,0:T(1,128)S(1)} %broadcast_in_dim.22), channel_id=1, replica_groups=mesh['kv_0'=8,'kv_1'=4,'tp_0'=4,'tp_1'=2] {'kv_0','kv_1'}, dimensions={0} | all-to-all | bytes 8192 | tf_op jit(solution)/shard_map/all_to_all | solution.py:20
  103.5 0.1 slice_multiply_fusion.3
  103.6 0.0 copy-done.5
  103.6 0.0 copy-done.6
  103.6 0.1 add_convert_fusion.1
  103.6 9.1 %all_to_all.75 = bf16[8,16,8]{1,2,0:T(8,128)(2,1)S(1)} all-to-all(bf16[8,16,8]{1,2,0:T(8,128)(2,1)S(1)} %broadcast_in_dim.23), channel_id=1, replica_groups=mesh['kv_0'=8,'kv_1'=4,'tp_0'=4,'tp_1'=2] {'tp_0','tp_1'}, dimensions={0} | all-to-all | bytes 4096 | tf_op jit(solution)/shard_map/all_to_all | solution.py:20
  112.8 0.0 copy-done.2
  112.8 0.2 fusion.7
  112.9 0.1 all_to_all.58
  113.0 11.9 %all_to_all.76 = f32[32,1,512]{2,1,0:T(1,128)S(1)} all-to-all(f32[32,1,512]{2,1,0:T(1,128)S(1)} %all_to_all.58), channel_id=1, replica_groups=mesh['kv_0'=8,'kv_1'=4,'tp_0'=4,'tp_1'=2] {'kv_0','kv_1'}, dimensions={0} | all-to-all | bytes 131072 | tf_op jit(solution)/shard_map/all_to_all | solution.py:86
  124.9 0.1 reduce_sum.134
  125.0 11.8 %all_to_all.77 = f32[32,1,512]{2,1,0:T(1,128)S(1)} all-to-all(f32[32,1,512]{2,1,0:T(1,128)S(1)} %broadcast_in_dim.24), channel_id=1, replica_groups=mesh['kv_0'=8,'kv_1'=4,'tp_0'=4,'tp_1'=2] {'kv_0','kv_1'}, dimensions={0} | all-to-all | bytes 131072 | tf_op jit(solution)/shard_map/all_to_all | solution.py:20
  136.8 0.2 convert_reduce_fusion
  137.1 0.0 copy-done.1
  137.1 0.2 fusion.55
  137.2 0.1 reshape.438
  137.3 9.9 %all_to_all.78 = f32[8,1,128]{2,1,0:T(1,128)S(1)} all-to-all(f32[8,1,128]{2,1,0:T(1,128)S(1)} %reshape.438), channel_id=1, replica_groups=mesh['kv_0'=8,'kv_1'=4,'tp_0'=4,'tp_1'=2] {'tp_0','tp_1'}, dimensions={0} | all-to-all | bytes 8192 | tf_op jit(solution)/shard_map/all_to_all | solution.py:86
  147.2 0.7 reduce.13
  147.9 0.1 reshape.439
  148.0 0.1 pad_maximum_fusion.3
  148.1 7.6 %all_to_all.79 = f32[8,1,32]{2,1,0:T(1,128)S(1)} all-to-all(f32[8,1,32]{2,1,0:T(1,128)S(1)} %broadcast_in_dim.25), channel_id=1, replica_groups=mesh['kv_0'=8,'kv_1'=4,'tp_0'=4,'tp_1'=2] {'tp_0','tp_1'}, dimensions={0} | all-to-all | bytes 2048 | tf_op jit(solution)/shard_map/all_to_all | solution.py:20
  155.8 11.6 %all_to_all.80 = f32[32,1,32]{2,1,0:T(1,128)S(1)} all-to-all(f32[32,1,32]{2,1,0:T(1,128)S(1)} %broadcast_in_dim.26), channel_id=1, replica_groups=mesh['kv_0'=8,'kv_1'=4,'tp_0'=4,'tp_1'=2] {'kv_0','kv_1'}, dimensions={0} | all-to-all | bytes 8192 | tf_op jit(solution)/shard_map/all_to_all | solution.py:20
  167.4 0.1 slice_multiply_fusion.2
  167.5 0.7 add_convert_fusion
  (61 shorter events, 0.8 us)
Async XLA Ops:
  0.0 48.7 %copy-start = (bf16[16,1,512,128]{3,2,1,0:T(8,128)(2,1)S(1)}, bf16[16,1,512,128]{3,2,1,0:T(8,128)(2,1)}, u32[]{:S(2)}) copy-start(bf16[16,1,512,128]{3,2,1,0:T(8,128)(2,1)} %param.27) | copy-start | bytes 6291460
  1.4 11.1 %all-to-all-start = ((bf16[8,16,8]{1,2,0:T(8,128)(2,1)}), bf16[8,16,8]{1,2,0:T(8,128)(2,1)S(1)}, u32[]{:S(2)}, u32[]{:S(2)}) async-start(bf16[8,16,8]{1,2,0:T(8,128)(2,1)} %broadcast_in_dim.18), calls=%async_computation | async-start | bytes 32768 | tf_op jit(solution)/shard_map/all_to_all | solution.py:20
  16.5 32.9 %copy-start.3 = (f32[16,1,512]{2,1,0:T(1,128)S(1)}, f32[16,1,512]{2,1,0:T(1,128)}, u32[]{:S(2)}) copy-start(f32[16,1,512]{2,1,0:T(1,128)} %param.29) | copy-start | bytes 98308
  48.7 1.6 copy-start.9
  50.3 20.8 %copy-start.10 = (bf16[128,64]{0,1:T(8,128)(2,1)S(1)}, bf16[128,64]{0,1:T(8,128)(2,1)}, u32[]{:S(2)}) copy-start(bf16[128,64]{0,1:T(8,128)(2,1)} %param.20) | copy-start | bytes 49156
  50.7 32.5 %copy-start.4 = (bf16[16,8]{0,1:T(8,128)(2,1)S(1)}, bf16[16,8]{0,1:T(8,128)(2,1)}, u32[]{:S(2)}) copy-start(bf16[16,8]{0,1:T(8,128)(2,1)} %param.15) | copy-start | bytes 772
  50.7 52.9 %copy-start.5 = (f32[8]{0:T(128)S(1)}, f32[8]{0:T(128)}, u32[]{:S(2)}) copy-start(f32[8]{0:T(128)} %param.22) | copy-start | bytes 100
  50.7 52.9 %copy-start.6 = (f32[8]{0:T(128)S(1)}, f32[8]{0:T(128)}, u32[]{:S(2)}) copy-start(f32[8]{0:T(128)} %param.21) | copy-start | bytes 100
  50.7 62.1 %copy-start.2 = (bf16[64,1024]{1,0:T(8,128)(2,1)S(1)}, bf16[64,1024]{1,0:T(8,128)(2,1)}, u32[]{:S(2)}) copy-start(bf16[64,1024]{1,0:T(8,128)(2,1)} %param.25) | copy-start | bytes 393220
  51.5 85.5 %copy-start.1 = (bf16[1024,64]{0,1:T(8,128)(2,1)S(1)}, bf16[1024,64]{0,1:T(8,128)(2,1)}, u32[]{:S(2)}) copy-start(bf16[1024,64]{0,1:T(8,128)(2,1)} %param.26) | copy-start | bytes 393220
  51.5 116.0 %copy-start.7 = (f32[8]{0:T(128)S(1)}, f32[8]{0:T(128)}, u32[]{:S(2)}) copy-start(f32[8]{0:T(128)} %param.24) | copy-start | bytes 100
  51.5 116.0 %copy-start.8 = (f32[8]{0:T(128)S(1)}, f32[8]{0:T(128)}, u32[]{:S(2)}) copy-start(f32[8]{0:T(128)} %param.23) | copy-start | bytes 100
  51.5 18.6 %all-to-all-start.2 = ((f32[32,18,128]{2,1,0:T(8,128)}), f32[32,18,128]{2,1,0:T(8,128)S(1)}, u32[]{:S(2)}, u32[]{:S(2)}) async-start(f32[32,18,128]{2,1,0:T(8,128)} %broadcast_in_dim.20), calls=%async_computation.2 | async-start | bytes 786432 | tf_op jit(solution)/shard_map/all_to_all | solution.py:20
where the time goes:
time: 169 us; the launch traced here: 168 us
  blocking collectives  124 us (73%)
  waiting for transfers between devices  17.1 us (10%)
  starting transfers between devices  12.4 us (7%)
  matrix products  5.13 us (3%)
  other arithmetic  4.51 us (3%)
  local copies, waits for them, and re-layouts  4.29 us (3%)
    all_to_all x7, blocking collectives, from_everyone(): lax.all_to_all(jnp.broadcast_to(shard[None], (length, *shard.shape)), axi...  92 us
    all_to_all x3, blocking collectives, sent_and_summed(): tiles = lax.all_to_all(split_up(shard, dim, length), axis, 0, 0, tiled=True)  32.4 us
    all_to_all x2, waiting for transfers between devices, from_everyone(): lax.all_to_all(jnp.broadcast_to(shard[None], (length, *shard.shape)), axi...  17.1 us
    all_to_all x2, starting transfers between devices, from_everyone(): lax.all_to_all(jnp.broadcast_to(shard[None], (length, *shard.shape)), axi...  12.4 us
  transfers between devices with their start and end apart: 2, of which 2 were waited for; matrix products, arithmetic and copies ran while one was open for 0% of the time, Pallas kernels for 0%

commit v1 on v0

v1 whole, which is shorter than its diff:
```python
import jax
import jax.numpy as jnp
from jax import lax
from jax.experimental import pallas as pl
from jax.experimental.pallas import tpu as pltpu
from jax.sharding import Mesh
from jax.sharding import PartitionSpec as P

D = 2048
HEAD_DIM = 128
B = 16
POS = 512
NZ, NX, NY, NC = 8, 4, 4, 2
NKV, NTP = NZ * NX, NY * NC
ROOT2 = 1.4142135623730951
EPS = 1e-05
SCALE = HEAD_DIM**-0.5
F32 = jnp.float32
BF16 = jnp.bfloat16
MESH = pl.DeviceIdType.MESH


def body(
    tokens, w_query, w_key, w_value, w_forget, w_out, mix_gain, mix_bias, ffn_gain, ffn_bias,
    w_up, w_down, keys, values, gates,
    out,
    tok_v, gain_v, bias_v, fgain_v, fbias_v, wq_v, wkv_v, wf_v, wo_v, wup_v, wdn_v, k_v, v_v, cg_v,
    stage, plane, q_buf, kvg_send, kvg_buf, gwb_send, gwb_buf, accx, stx, accz, stz, head_buf,
    mst, up_send, up_buf, hid_buf, hid_f, down_buf, ost,
    load_sem, k_sem, v_sem, send_sem, recv_sem,
):
    z, x, y, c = (lax.axis_index(a) for a in ("z", "x", "y", "c"))
    kv = z * NX + x
    tp = y * NC + c
    slot = x * NTP + tp

    barrier = pltpu.get_barrier_semaphore()

    def plane_peer(i):
        t = i // NTP
        r = i % NTP
        px = (x + NX - 1 - t + NX) % NX
        py = (y + NY - 1 - r // NC + NY) % NY
        pc = (c + NC - 1 - r % NC) % NC
        return {"x": px, "y": py, "c": pc}

    def greet_plane(i, carry):
        pl.semaphore_signal(barrier, inc=1, device_id=plane_peer(i), device_id_type=MESH)
        return carry

    def greet_line(i, carry):
        pl.semaphore_signal(
            barrier, inc=1, device_id={"z": (z + 1 + i) % NZ}, device_id_type=MESH
        )
        return carry

    lax.fori_loop(0, NZ - 1, greet_line, 0)
    lax.fori_loop(0, NX * NTP - 1, greet_plane, 0)

    loads = []

    def load(src, dst, sem):
        copy = pltpu.make_async_copy(src, dst, sem)
        copy.start()
        return copy

    first = [
        load(tokens, tok_v, load_sem.at[0]),
        load(mix_gain, gain_v, load_sem.at[1]),
        load(mix_bias, bias_v, load_sem.at[2]),
    ]
    load_q = load(w_query, wq_v.at[x], load_sem.at[3])
    load_k = load(w_key, wkv_v.at[x, 0], load_sem.at[4])
    load_v = load(w_value, wkv_v.at[x, 1], load_sem.at[5])
    load_f = load(w_forget.at[pl.ds(z * NX * 64, NX * 64)], wf_v, load_sem.at[6])
    load_o = load(w_out, wo_v, load_sem.at[7])
    load_up = load(w_up, wup_v, load_sem.at[8])
    load_fg = load(ffn_gain, fgain_v, load_sem.at[9])
    load_fb = load(ffn_bias, fbias_v, load_sem.at[10])
    load_cg = load(gates, cg_v, load_sem.at[11])
    load_key = [load(keys.at[pl.ds(4 * i, 4)], k_v.at[pl.ds(4 * i, 4)], k_sem.at[i]) for i in range(4)]
    load_val = [load(values.at[pl.ds(4 * i, 4)], v_v.at[pl.ds(4 * i, 4)], v_sem.at[i]) for i in range(4)]
    load_dn = load(w_down, wdn_v, load_sem.at[12])

    lane = lax.broadcasted_iota(jnp.int32, (B, 128), 1)
    row = lax.broadcasted_iota(jnp.int32, (B, 128), 0)
    lane1 = lax.broadcasted_iota(jnp.int32, (1, 128), 1)
    diag = row == lane
    diag16 = row == lane - B

    def to_row(col, mask):
        return jnp.sum(jnp.where(mask, jnp.broadcast_to(col, (B, 128)), 0.0), axis=0, keepdims=True)

    def to_col(line):
        return jnp.sum(
            jnp.where(diag, jnp.broadcast_to(line, (B, 128)), 0.0), axis=1, keepdims=True
        )

    for copy in first:
        copy.wait()
    stage[...] = jnp.zeros((128, 128), F32)
    stage[0:B, 0:8] = tok_v[...].astype(F32)
    stage[B : B + 1, 0:8] = gain_v[...]
    stage[B + 1 : B + 2, 0:8] = bias_v[...]
    plane[slot] = stage[...].T[0:8, :]
    load_q.wait()
    load_k.wait()
    load_v.wait()

    pl.semaphore_wait(barrier, NZ - 1 + NX * NTP - 1)

    def push(src, dst, phase, peer):
        pltpu.make_async_remote_copy(
            src_ref=src,
            dst_ref=dst,
            send_sem=send_sem.at[phase],
            recv_sem=recv_sem.at[phase],
            device_id=peer,
            device_id_type=MESH,
        ).start()

    def received(ref, count, phase):
        part = ref.at[pl.ds(0, count)]
        pltpu.make_async_copy(part, part, recv_sem.at[phase]).wait()

    def sent(ref, count, phase):
        part = ref.at[pl.ds(0, count)]
        pltpu.make_async_copy(part, part, send_sem.at[phase]).wait()

    def line_peer(i):
        step = (i + 1) // 2 * (2 * (i % 2) - 1) + 4
        return (z + step + NZ) % NZ

    def kv_peer(i):
        t = i // NX
        step = (t + 1) // 2 * (2 * (t % 2) - 1) + 4
        return (z + step + NZ) % NZ, (x + NX - 1 - i % NX) % NX

    def loop(count, f):
        def step(i, carry):
            f(i)
            return carry

        lax.fori_loop(0, count, step, 0)

    loop(NX * NTP - 1, lambda i: push(plane.at[slot], plane.at[slot], 0, plane_peer(i)))
    loop(NX - 1, lambda i: push(wq_v.at[x], wq_v.at[x], 1, {"x": (x + NX - 1 - i) % NX}))
    loop(NX - 1, lambda i: push(wkv_v.at[x], wkv_v.at[x], 2, {"x": (x + NX - 1 - i) % NX}))

    received(plane, NX * NTP - 1, 0)
    spread = plane[...].reshape(NX * NTP * 8, 128).T
    tok = spread[0:B, :].astype(BF16)
    received(wq_v, NX - 1, 1)
    q_buf[z] = jnp.dot(tok, wq_v[...].reshape(NX * 64, HEAD_DIM), preferred_element_type=F32)
    loop(
        NZ - 1, lambda i: push(q_buf.at[z], q_buf.at[z], 3, {"z": line_peer(i)})
    )
    received(wkv_v, NX - 1, 2)
    load_f.wait()
    key_part = jnp.dot(tok, wkv_v[:, 0].reshape(NX * 64, HEAD_DIM), preferred_element_type=F32)
    value_part = jnp.dot(tok, wkv_v[:, 1].reshape(NX * 64, HEAD_DIM), preferred_element_type=F32)
    gate_part = jnp.dot(tok, wf_v[...], preferred_element_type=F32)
    lane8 = lax.broadcasted_iota(jnp.int32, (B, 8), 1)
    gate_part = jnp.sum(jnp.where(lane8 == tp, gate_part, 0.0), axis=1, keepdims=True)
    gate_part = jnp.broadcast_to(gate_part, (B, 128))
    for i in range(NZ):
        kvg_send[i, :, 0:128] = key_part[2 * i : 2 * i + 2, :]
        kvg_send[i, :, 128:256] = value_part[2 * i : 2 * i + 2, :]
        kvg_send[i, :, 256:384] = gate_part[2 * i : 2 * i + 2, :]
    kvg_buf[z] = kvg_send[z]

    def push_kvg(i):
        pz = line_peer(i)
        push(kvg_send.at[pz], kvg_buf.at[z], 4, {"z": pz})

    loop(NZ - 1, push_kvg)

    own = jnp.where(x >= 2, spread[0:24, 128:256], spread[0:24, 0:128])
    own = jnp.where(x % 2 == 1, pltpu.roll(own, 64, 1), own)
    tok_own = own[0:B, :]
    gain_own = own[B : B + 1, :]
    bias_own = own[B + 1 : B + 2, :]

    load_up.wait()
    both = jnp.concatenate([gain_own, bias_own], axis=0)[:, 0:64]
    both_hi = both.astype(BF16)
    both_lo = (both - both_hi.astype(F32)).astype(BF16)
    gwb = jnp.dot(
        jnp.concatenate([both_hi.astype(F32), both_lo.astype(F32)], axis=0).astype(BF16),
        wup_v[...],
        preferred_element_type=F32,
    )
    gwb = gwb[0:2, :] + gwb[2:4, :]
    for h in range(2):
        for j in range(4):
            at = (h * 4 + j) * 128
            gwb_send[h, j : j + 1, :] = gwb[0:1, at : at + 128]
            gwb_send[h, 4 + j : 5 + j, :] = gwb[1:2, at : at + 128]
    gwb_buf[kv] = gwb_send[kv % 2]

    received(q_buf, NZ - 1, 3)
    query = jnp.sum(q_buf[...], axis=0).astype(BF16)

    def push_gwb(i):
        pz, px = kv_peer(i)
        push(gwb_send.at[px % 2], gwb_buf.at[kv], 5, {"z": pz, "x": px})

    loop(NKV - 1, push_gwb)

    load_cg.wait()
    row_pos = lax.broadcasted_iota(jnp.int32, (B, POS), 0)
    scores = jnp.zeros((B, POS), F32)
    for b in range(B):
        if b % 4 == 0:
            load_key[b // 4].wait()
        part = lax.dot_general(
            query, k_v[b], (((1,), (1,)), ((), ())), preferred_element_type=F32
        )
        scores = jnp.where(row_pos == b, part, scores)
    gates_here = jnp.concatenate([cg_v[b] for b in range(B)], axis=0)
    scores = scores * SCALE + gates_here
    received(kvg_buf, NZ - 1, 4)
    kvg = jnp.sum(kvg_buf[...], axis=0)
    kvg16 = jnp.where(
        lax.broadcasted_iota(jnp.int32, (B, 384), 0) % 2 == 0,
        jnp.broadcast_to(kvg[0:1, :], (B, 384)),
        jnp.broadcast_to(kvg[1:2, :], (B, 384)),
    )
    key_new = kvg16[:, 0:128].astype(BF16).astype(F32)
    value_new = kvg16[:, 128:256].astype(BF16).astype(F32)
    gate_sum = kvg16[:, 256:257]
    log_forget = jnp.minimum(gate_sum, 0.0) - jnp.log1p(jnp.exp(-jnp.abs(gate_sum)))
    own_score = jnp.sum(query.astype(F32) * key_new, axis=1, keepdims=True) * SCALE - log_forget
    mine = (row[:, 0:1] // 2 == z) & (x == 0)
    own_score = jnp.where(mine, own_score, -1e30)
    value_new = jnp.where(mine, value_new, 0.0)
    peak = jnp.maximum(jnp.max(scores, axis=1, keepdims=True), own_score)
    weights = jnp.exp(scores - peak)
    own_weight = jnp.exp(own_score - peak)
    total = jnp.sum(weights, axis=1, keepdims=True) + own_weight
    weights = weights.astype(BF16)
    acc = jnp.zeros((B, HEAD_DIM), F32)
    for b in range(B):
        if b % 4 == 0:
            load_val[b // 4].wait()
        part = jnp.dot(weights, v_v[b], preferred_element_type=F32)
        acc = jnp.where(row == b, part, acc)
    acc = acc + own_weight * value_new

    stx[x] = jnp.concatenate([to_row(peak, diag), to_row(total, diag)], axis=0)
    loop(NX - 1, lambda i: push(stx.at[x], stx.at[x], 7, {"x": (x + NX - 1 - i) % NX}))
    accx[x] = acc
    loop(NX - 1, lambda i: push(accx.at[x], accx.at[x], 6, {"x": (x + NX - 1 - i) % NX}))

    def combine(acc_ref, st_ref, count, acc_phase, st_phase):
        received(st_ref, count - 1, st_phase)
        peaks = [st_ref[i, 0:1, :] for i in range(count)]
        peak = peaks[0]
        for p in peaks[1:]:
            peak = jnp.maximum(peak, p)
        factors = [jnp.exp(p - peak) for p in peaks]
        total = factors[0] * st_ref[0, 1:2, :]
        for i in range(1, count):
            total = total + factors[i] * st_ref[i, 1:2, :]
        cols = [to_col(f) for f in factors]
        received(acc_ref, count - 1, acc_phase)
        acc = cols[0] * acc_ref[0]
        for i in range(1, count):
            acc = acc + cols[i] * acc_ref[i]
        return peak, total, acc

    load_o.wait()
    w_out2 = jnp.concatenate([wo_v[...], wo_v[...]], axis=1)
    load_dn.wait()
    w_down2 = jnp.concatenate([wdn_v[...], wdn_v[...]], axis=1)

    peak, total, acc = combine(accx, stx, NX, 6, 7)
    stz[z] = jnp.concatenate([peak, total], axis=0)
    loop(NZ - 1, lambda i: push(stz.at[z], stz.at[z], 9, {"z": line_peer(i)}))
    accz[z] = acc
    loop(NZ - 1, lambda i: push(accz.at[z], accz.at[z], 8, {"z": line_peer(i)}))
    peak, total, acc = combine(accz, stz, NZ, 8, 9)
    attended = (acc / to_col(total)).astype(BF16)

    lane_half = lax.broadcasted_iota(jnp.int32, (8, 128), 1) < 64

    def tp_peer(i):
        return {"y": (y + NY - 1 - i // NC) % NY, "c": (c + NC - 1 - i % NC) % NC}

    def tp_sum(terms, ref, phase):
        ref[tp] = jnp.where(lane_half, terms[0:8, :], terms[8:16, :])
        loop(NTP - 1, lambda i: push(ref.at[tp], ref.at[tp], phase, tp_peer(i)))
        received(ref, NTP - 1, phase)
        summed = jnp.sum(ref[...], axis=0)
        return jnp.concatenate([summed, pltpu.roll(summed, 64, 1)], axis=0)

    head_terms = tp_sum(jnp.dot(attended, w_out2, preferred_element_type=F32), head_buf, 10)
    mixed = jnp.where(lane < 64, ROOT2 * tok_own + head_terms, 0.0)

    def push_stats(values, ref, phase):
        sums = jnp.sum(values, axis=1, keepdims=True)
        squares = jnp.sum(values * values, axis=1, keepdims=True)
        ref[kv] = to_row(sums, diag) + to_row(squares, diag16)

        def push_one(i):
            pz, px = kv_peer(i)
            push(ref.at[kv], ref.at[kv], phase, {"z": pz, "x": px})

        loop(NKV - 1, push_one)

    def stats(ref, phase):
        received(ref, NKV - 1, phase)
        line = jnp.sum(ref[...], axis=0)
        mean = line / D
        var = pltpu.roll(line, 128 - B, 1) / D - mean * mean
        return mean, lax.rsqrt(var + EPS)

    push_stats(mixed, mst, 11)

    scaled = mixed * jnp.broadcast_to(gain_own, (B, 128))
    scaled_hi = scaled.astype(BF16)
    scaled_lo = (scaled - scaled_hi.astype(F32)).astype(BF16)
    up = jnp.dot(
        jnp.concatenate([scaled_hi, scaled_lo], axis=0)[:, 0:64],
        wup_v[...],
        preferred_element_type=F32,
    )
    up = up[0:B, :] + up[B : 2 * B, :]
    for h in range(2):
        for j in range(4):
            at = (h * 4 + j) * 128
            up_send[:, h, j, :] = up[:, at : at + 128]
    up_buf[kv] = up_send[kv // 2, kv % 2]

    def push_up(i):
        pz, px = kv_peer(i)
        push(up_send.at[2 * pz + px // 2, px % 2], up_buf.at[kv], 12, {"z": pz, "x": px})

    loop(NKV - 1, push_up)
    received(gwb_buf, NKV - 1, 5)
    gwb = jnp.sum(gwb_buf[...], axis=0)
    mean, rstd = stats(mst, 11)
    pick = lane1 == kv // 2
    mean_here = jnp.sum(jnp.where(pick, mean, 0.0), axis=1, keepdims=True)
    rstd_here = jnp.sum(jnp.where(pick, rstd, 0.0), axis=1, keepdims=True)
    received(up_buf, NKV - 1, 12)
    up_sum = jnp.sum(up_buf[...], axis=0)
    up_row = rstd_here * (up_sum - mean_here * gwb[0:4, :]) + gwb[4:8, :]
    hidden = jnp.square(jnp.maximum(up_row, 0.0)).astype(BF16)
    hid_buf[kv] = hidden

    def push_hidden(i):
        pz, px = kv_peer(i)
        push(hid_buf.at[kv], hid_buf.at[kv], 13, {"z": pz, "x": px})

    loop(NKV - 1, push_hidden)

    normed = (mixed - to_col(mean)) * to_col(rstd) * gain_own + bias_own
    normed = normed.astype(BF16).astype(F32)
    fgain = fgain_v
    received(hid_buf, NKV - 1, 13)
    hid_f[...] = hid_buf[...].astype(F32).reshape(B, 2, 4, 128)
    hidden_all = jnp.concatenate(
        [hid_f[:, h, j, :].astype(BF16) for h in range(2) for j in range(4)], axis=1
    )
    down_terms = tp_sum(jnp.dot(hidden_all, w_down2, preferred_element_type=F32), down_buf, 14)
    outer = jnp.where(lane < 64, ROOT2 * normed + down_terms, 0.0)
    push_stats(outer, ost, 15)
    outer = pltpu.roll(outer, (128 - 8 * tp) % 128, 1)[:, 0:8]
    load_fg.wait()
    load_fb.wait()

    sent(plane, NX * NTP - 1, 0)
    sent(wq_v, NX - 1, 1)
    sent(wkv_v, NX - 1, 2)
    sent(q_buf, NZ - 1, 3)
    sent(kvg_buf, NZ - 1, 4)
    sent(gwb_buf, NKV - 1, 5)
    sent(accx, NX - 1, 6)
    sent(stx, NX - 1, 7)
    sent(accz, NZ - 1, 8)
    sent(stz, NZ - 1, 9)
    sent(head_buf, NTP - 1, 10)
    sent(mst, NKV - 1, 11)
    sent(up_buf, NKV - 1, 12)
    sent(hid_buf, NKV - 1, 13)
    sent(down_buf, NTP - 1, 14)
    sent(ost, NKV - 1, 15)
    mean, rstd = stats(ost, 15)
    result = (outer - to_col(mean)) * to_col(rstd) * fgain_v[...] + fbias_v[...]
    out[...] = result.astype(BF16)


def shards(
    tokens, w_query, w_key, w_value, w_forget, w_out, mix_gain, mix_bias, ffn_gain, ffn_bias,
    w_up, down_weight, cache_keys, cache_values, cum_gates,
):
    vmem = pltpu.VMEM
    scratch = [
        vmem((B, 8), BF16),
        vmem((1, 8), F32),
        vmem((1, 8), F32),
        vmem((1, 8), F32),
        vmem((1, 8), F32),
        vmem((NX, 64, 128), BF16),
        vmem((NX, 2, 64, 128), BF16),
        vmem((NX * 64, 8), BF16),
        vmem((128, 64), BF16),
        vmem((64, 1024), BF16),
        vmem((1024, 64), BF16),
        vmem((B, POS, 128), BF16),
        vmem((B, POS, 128), BF16),
        vmem((B, 1, POS), F32),
        vmem((128, 128), F32),
        vmem((NX * NTP, 8, 128), F32),
        vmem((NZ, B, 128), F32),
        vmem((NZ, 2, 384), F32),
        vmem((NZ, 2, 384), F32),
        vmem((2, 8, 128), F32),
        vmem((NKV, 8, 128), F32),
        vmem((NX, B, 128), F32),
        vmem((NX, 2, 128), F32),
        vmem((NZ, B, 128), F32),
        vmem((NZ, 2, 128), F32),
        vmem((NTP, 8, 128), F32),
        vmem((NKV, 1, 128), F32),
        vmem((B, 2, 4, 128), F32),
        vmem((NKV, 4, 128), F32),
        vmem((NKV, 4, 128), BF16),
        vmem((B, 2, 4, 128), F32),
        vmem((NTP, 8, 128), F32),
        vmem((NKV, 1, 128), F32),
        pltpu.SemaphoreType.DMA((13,)),
        pltpu.SemaphoreType.DMA((4,)),
        pltpu.SemaphoreType.DMA((4,)),
        pltpu.SemaphoreType.DMA((16,)),
        pltpu.SemaphoreType.DMA((16,)),
    ]
    any_space = pl.BlockSpec(memory_space=pl.ANY)
    return pl.pallas_call(
        body,
        out_shape=jax.ShapeDtypeStruct((B, 8), BF16),
        in_specs=[any_space] * 15,
        out_specs=pl.BlockSpec(memory_space=pltpu.VMEM),
        scratch_shapes=scratch,
        compiler_params=pltpu.CompilerParams(
            collective_id=0, has_side_effects=True, vmem_limit_bytes=48 * 1024 * 1024
        ),
        name="step",
    )(
        tokens, w_query, w_key, w_value, w_forget, w_out,
        mix_gain.reshape(1, 8), mix_bias.reshape(1, 8),
        ffn_gain.reshape(1, 8), ffn_bias.reshape(1, 8),
        w_up, down_weight,
        cache_keys.reshape(B, POS, HEAD_DIM), cache_values.reshape(B, POS, HEAD_DIM),
        cum_gates,
    )


def solution(mesh):
    finer = Mesh(mesh.devices.reshape(NZ, NX, NY, NC), ("z", "x", "y", "c"))
    kv, tp, both = ("z", "x"), ("y", "c"), ("z", "x", "y", "c")
    return jax.shard_map(
        shards,
        mesh=finer,
        in_specs=(
            P(None, both), P(kv, tp), P(kv, tp), P(kv, tp), P(), P(tp, kv),
            P(both), P(both), P(both), P(both),
            P(kv, tp), P(tp, kv),
            P(None, tp, kv, None), P(None, tp, kv, None), P(None, tp, kv),
        ),
        out_specs=P(None, both),
        check_vma=False,
    )
```

time: 169 us -> 72.2 us (0.43)
  blocking collectives: 124 us -> 0 us
  Pallas kernels: 0 us -> 57.6 us
  waiting for transfers between devices: 17.1 us -> 0 us
  starting transfers between devices: 12.4 us -> 0 us
  local copies, waits for them, and re-layouts: 4.29 us -> 14 us
  matrix products: 5.13 us -> 0 us
  other arithmetic: 4.51 us -> 0 us
    all_to_all x10 -> x0, blocking collectives: 124 us -> none  [the longest x7 92 us: from_everyone(): lax.all_to_all(jnp.broadcast_to(shard[None], (length, *shard.shape)), axi...]
    pallas_call x0 -> x1, Pallas kernels: none -> 57.6 us  [shards(): pl.pallas_call(body, out_shape=jax.ShapeDtypeStruct((B, 8), BF16), in_spe...]
    all_to_all x2 -> x0, waiting for transfers between devices: 17.1 us -> none  [from_everyone(): lax.all_to_all(jnp.broadcast_to(shard[None], (length, *shard.shape)), axi...]
    unnamed x26, local copies, waits for them, and re-layouts: 0.65 us -> 13.3 us
    all_to_all x2 -> x0, starting transfers between devices: 12.4 us -> none  [from_everyone(): lax.all_to_all(jnp.broadcast_to(shard[None], (length, *shard.shape)), axi...]
    dot_general x9 -> x0, matrix products: 5.13 us -> none  [the longest x1 0.89 us: shards(): jnp.dot(local_columns, w_key, preferred_element_type=jnp.float32)]
    broadcast_in_dim x9 -> x0, local copies, waits for them, and re-layouts: 2.69 us -> none  [from_everyone(): jnp.broadcast_to(shard[None], (length, *shard.shape))]
  transfers between devices with their start and end apart: 2 -> 0, of which waited for: 2 -> 0; matrix products, arithmetic and copies ran while one was open for 0% -> 0% of each run, Pallas kernels for 0% -> 0%
where the time goes in v1:
time: 72.2 us; the launch traced here: 71.6 us
  Pallas kernels  57.6 us (80%)
  local copies, waits for them, and re-layouts  14 us (19%)
    pallas_call x1, Pallas kernels, shards(): pl.pallas_call(body, out_shape=jax.ShapeDtypeStruct((B, 8), BF16), in_spe...  57.6 us
    unnamed x26, local copies, waits for them, and re-layouts  13.3 us

profile of v1, /device:TPU:1, one launch (start us, length us, event | category | flops | bytes accessed | tf_op | source)
XLA Modules:
  0.0 71.6 jit_solution(3536937394349505818)
XLA Ops:
  0.0 0.8 %copy.16.tokens = bf16[16,8]{1,0:T(8,128)(2,1)S(1)} copy(bf16[16,8]{0,1:T(8,128)(2,1)} %param.15) | data formatting | bytes 512 | tf_op args[0]
  0.8 0.8 %copy.18.w_out = bf16[128,64]{1,0:T(8,128)(2,1)S(1)} copy(bf16[128,64]{0,1:T(8,128)(2,1)} %param.20) | data formatting | bytes 32768 | tf_op args[5]
  1.6 1.1 %copy.19.w_down = bf16[1024,64]{1,0:T(8,128)(2,1)S(1)} copy(bf16[1024,64]{0,1:T(8,128)(2,1)} %param.26) | data formatting | bytes 262144 | tf_op args[11]
  2.7 1.0 %copy.17.w_forget = bf16[2048,8]{1,0:T(8,128)(2,1)S(1)} copy(bf16[2048,8]{0,1:T(8,128)(2,1)} %param.19) | data formatting | bytes 65536 | tf_op args[4]
  3.7 0.0 copy-start
  3.7 1.6 %copy-done = bf16[16,1,512,128]{3,2,1,0:T(8,128)(2,1)S(1)} copy-done((bf16[16,1,512,128]{3,2,1,0:T(8,128)(2,1)S(1)}, bf16[16,1,512,128]{3,2,1,0:T(8,128)(2,1)}, u32[]{:S(2)}) %copy-start) | copy-done | bytes 2097176
  5.3 0.0 copy-start.1
  5.3 1.6 %copy-done.1 = bf16[16,1,512,128]{3,2,1,0:T(8,128)(2,1)S(1)} copy-done((bf16[16,1,512,128]{3,2,1,0:T(8,128)(2,1)S(1)}, bf16[16,1,512,128]{3,2,1,0:T(8,128)(2,1)}, u32[]{:S(2)}) %copy-start.1) | copy-done | bytes 2097176
  6.9 0.0 copy-start.2
  6.9 0.9 %copy-done.2 = bf16[64,1024]{1,0:T(8,128)(2,1)S(1)} copy-done((bf16[64,1024]{1,0:T(8,128)(2,1)S(1)}, bf16[64,1024]{1,0:T(8,128)(2,1)}, u32[]{:S(2)}) %copy-start.2) | copy-done | bytes 131096
  7.8 0.0 copy-start.3
  7.8 0.8 %copy-done.3 = f32[16,1,512]{2,1,0:T(1,128)S(1)} copy-done((f32[16,1,512]{2,1,0:T(1,128)S(1)}, f32[16,1,512]{2,1,0:T(1,128)}, u32[]{:S(2)}) %copy-start.3) | copy-done | bytes 32792
  8.6 0.0 copy-start.4
  8.6 0.7 copy-done.4
  9.3 0.0 copy-start.5
  9.3 0.7 copy-done.5
  10.0 0.0 copy-start.6
  10.0 0.7 copy-done.6
  10.7 0.0 copy-start.7
  10.7 0.7 copy-done.7
  11.4 0.0 copy-start.8
  11.4 0.7 copy-done.8
  12.0 0.0 copy-start.9
  12.0 0.7 copy-done.9
  12.7 0.0 copy-start.10
  12.7 0.7 copy-done.10
  13.3 57.6 %step.1 = bf16[16,8]{1,0:T(8,128)(2,1)S(1)} custom-call(bf16[16,8]{1,0:T(8,128)(2,1)S(1)} %copy.16.tokens, bf16[64,128]{1,0:T(8,128)(2,1)S(1)} %copy-done.4, bf16[64,128]{1,0:T(8,128)(2,1)S(1)} %copy-done.5, bf16[64,128]{1,0:T(8,128)(2,1)S(1)} %copy-done.6, bf16[2048,8]{1,0:T(8,128)(2,1)S(1)} %copy.17.w_forget, bf16[128,64]{1,0:T(8,128)(2,1)S(1)} %copy.18.w_out, ...), custom_call_target="tpu_custom_call" | custom-call | tf_op jit(solution)/shard_map/step/pallas_call | solution.py:440
  71.0 0.7 copy.20
Async XLA Ops:
  3.7 1.6 %copy-start = (bf16[16,1,512,128]{3,2,1,0:T(8,128)(2,1)S(1)}, bf16[16,1,512,128]{3,2,1,0:T(8,128)(2,1)}, u32[]{:S(2)}) copy-start(bf16[16,1,512,128]{3,2,1,0:T(8,128)(2,1)} %param.27) | copy-start | bytes 6291460
  5.3 1.6 %copy-start.1 = (bf16[16,1,512,128]{3,2,1,0:T(8,128)(2,1)S(1)}, bf16[16,1,512,128]{3,2,1,0:T(8,128)(2,1)}, u32[]{:S(2)}) copy-start(bf16[16,1,512,128]{3,2,1,0:T(8,128)(2,1)} %param.28) | copy-start | bytes 6291460
  6.9 0.9 %copy-start.2 = (bf16[64,1024]{1,0:T(8,128)(2,1)S(1)}, bf16[64,1024]{1,0:T(8,128)(2,1)}, u32[]{:S(2)}) copy-start(bf16[64,1024]{1,0:T(8,128)(2,1)} %w_up.1) | copy-start | bytes 393220
  7.8 0.8 %copy-start.3 = (f32[16,1,512]{2,1,0:T(1,128)S(1)}, f32[16,1,512]{2,1,0:T(1,128)}, u32[]{:S(2)}) copy-start(f32[16,1,512]{2,1,0:T(1,128)} %gates.1) | copy-start | bytes 98308
  8.6 0.7 %copy-start.4 = (bf16[64,128]{1,0:T(8,128)(2,1)S(1)}, bf16[64,128]{1,0:T(8,128)(2,1)}, u32[]{:S(2)}) copy-start(bf16[64,128]{1,0:T(8,128)(2,1)} %w_query.1) | copy-start | bytes 49156
  9.3 0.7 %copy-start.5 = (bf16[64,128]{1,0:T(8,128)(2,1)S(1)}, bf16[64,128]{1,0:T(8,128)(2,1)}, u32[]{:S(2)}) copy-start(bf16[64,128]{1,0:T(8,128)(2,1)} %w_key.1) | copy-start | bytes 49156
  10.0 0.7 %copy-start.6 = (bf16[64,128]{1,0:T(8,128)(2,1)S(1)}, bf16[64,128]{1,0:T(8,128)(2,1)}, u32[]{:S(2)}) copy-start(bf16[64,128]{1,0:T(8,128)(2,1)} %w_value.1) | copy-start | bytes 49156
  10.7 0.7 copy-start.7
  11.4 0.7 copy-start.8
  12.0 0.7 copy-start.9
  12.7 0.7 copy-start.10

commit v2 on v1

--- a/solution.py
+++ b/solution.py
@@ -20,13 +20,17 @@
 MESH = pl.DeviceIdType.MESH
 
 
+def across(a, b):
+    return lax.dot_general(a, b, (((1,), (1,)), ((), ())), preferred_element_type=F32)
+
+
 def body(
     tokens, w_query, w_key, w_value, w_forget, w_out, mix_gain, mix_bias, ffn_gain, ffn_bias,
     w_up, w_down, keys, values, gates,
     out,
     tok_v, gain_v, bias_v, fgain_v, fbias_v, wq_v, wkv_v, wf_v, wo_v, wup_v, wdn_v, k_v, v_v, cg_v,
     stage, plane, q_buf, kvg_send, kvg_buf, gwb_send, gwb_buf, accx, stx, accz, stz, head_buf,
-    mst, up_send, up_buf, hid_buf, hid_f, down_buf, ost,
+    mst, up_send, up_buf, hid_buf, hid_f, down_buf, ost, turned,
     load_sem, k_sem, v_sem, send_sem, recv_sem,
 ):
     z, x, y, c = (lax.axis_index(a) for a in ("z", "x", "y", "c"))
@@ -72,7 +76,7 @@
     load_q = load(w_query, wq_v.at[x], load_sem.at[3])
     load_k = load(w_key, wkv_v.at[x, 0], load_sem.at[4])
     load_v = load(w_value, wkv_v.at[x, 1], load_sem.at[5])
-    load_f = load(w_forget.at[pl.ds(z * NX * 64, NX * 64)], wf_v, load_sem.at[6])
+    load_f = load(w_forget.at[:, pl.ds(z * NX * 64, NX * 64)], wf_v, load_sem.at[6])
     load_o = load(w_out, wo_v, load_sem.at[7])
     load_up = load(w_up, wup_v, load_sem.at[8])
     load_fg = load(ffn_gain, fgain_v, load_sem.at[9])
@@ -98,11 +102,21 @@
 
     for copy in first:
         copy.wait()
-    stage[...] = jnp.zeros((128, 128), F32)
-    stage[0:B, 0:8] = tok_v[...].astype(F32)
-    stage[B : B + 1, 0:8] = gain_v[...]
-    stage[B + 1 : B + 2, 0:8] = bias_v[...]
-    plane[slot] = stage[...].T[0:8, :]
+    lane_8 = lax.broadcasted_iota(jnp.int32, (8, 128), 1)
+    diag_8 = lax.broadcasted_iota(jnp.int32, (8, 8), 0) == lax.broadcasted_iota(
+        jnp.int32, (8, 8), 1
+    )
+
+    def upright(line):
+        return jnp.sum(
+            jnp.where(diag_8, jnp.broadcast_to(line, (8, 8)), 0.0), axis=1, keepdims=True
+        )
+
+    stage[...] = jnp.where(
+        lane_8 == B, upright(gain_v[...]), jnp.where(lane_8 == B + 1, upright(bias_v[...]), 0.0)
+    )
+    stage[:, 0:B] = tok_v[...].astype(F32)
+    plane[slot] = stage[...]
     load_q.wait()
     load_k.wait()
     load_v.wait()
@@ -159,7 +173,7 @@
     load_f.wait()
     key_part = jnp.dot(tok, wkv_v[:, 0].reshape(NX * 64, HEAD_DIM), preferred_element_type=F32)
     value_part = jnp.dot(tok, wkv_v[:, 1].reshape(NX * 64, HEAD_DIM), preferred_element_type=F32)
-    gate_part = jnp.dot(tok, wf_v[...], preferred_element_type=F32)
+    gate_part = across(tok, wf_v[...])
     lane8 = lax.broadcasted_iota(jnp.int32, (B, 8), 1)
     gate_part = jnp.sum(jnp.where(lane8 == tp, gate_part, 0.0), axis=1, keepdims=True)
     gate_part = jnp.broadcast_to(gate_part, (B, 128))
@@ -213,9 +227,7 @@
     for b in range(B):
         if b % 4 == 0:
             load_key[b // 4].wait()
-        part = lax.dot_general(
-            query, k_v[b], (((1,), (1,)), ((), ())), preferred_element_type=F32
-        )
+        part = across(query, k_v[b])
         scores = jnp.where(row_pos == b, part, scores)
     gates_here = jnp.concatenate([cg_v[b] for b in range(B)], axis=0)
     scores = scores * SCALE + gates_here
@@ -270,9 +282,9 @@
         return peak, total, acc
 
     load_o.wait()
-    w_out2 = jnp.concatenate([wo_v[...], wo_v[...]], axis=1)
+    w_out2 = jnp.concatenate([wo_v[...], wo_v[...]], axis=0)
     load_dn.wait()
-    w_down2 = jnp.concatenate([wdn_v[...], wdn_v[...]], axis=1)
+    w_down2 = jnp.concatenate([wdn_v[...], wdn_v[...]], axis=0)
 
     peak, total, acc = combine(accx, stx, NX, 6, 7)
     stz[z] = jnp.concatenate([peak, total], axis=0)
@@ -294,7 +306,7 @@
         summed = jnp.sum(ref[...], axis=0)
         return jnp.concatenate([summed, pltpu.roll(summed, 64, 1)], axis=0)
 
-    head_terms = tp_sum(jnp.dot(attended, w_out2, preferred_element_type=F32), head_buf, 10)
+    head_terms = tp_sum(across(attended, w_out2), head_buf, 10)
     mixed = jnp.where(lane < 64, ROOT2 * tok_own + head_terms, 0.0)
 
     def push_stats(values, ref, phase):
@@ -357,18 +369,20 @@
 
     normed = (mixed - to_col(mean)) * to_col(rstd) * gain_own + bias_own
     normed = normed.astype(BF16).astype(F32)
-    fgain = fgain_v
     received(hid_buf, NKV - 1, 13)
     hid_f[...] = hid_buf[...].astype(F32).reshape(B, 2, 4, 128)
     hidden_all = jnp.concatenate(
         [hid_f[:, h, j, :].astype(BF16) for h in range(2) for j in range(4)], axis=1
     )
-    down_terms = tp_sum(jnp.dot(hidden_all, w_down2, preferred_element_type=F32), down_buf, 14)
+    down_terms = tp_sum(across(hidden_all, w_down2), down_buf, 14)
     outer = jnp.where(lane < 64, ROOT2 * normed + down_terms, 0.0)
     push_stats(outer, ost, 15)
-    outer = pltpu.roll(outer, (128 - 8 * tp) % 128, 1)[:, 0:8]
+    turned[...] = jnp.concatenate([outer, jnp.zeros((128 - B, 128), F32)], axis=0).T
+    outer = turned[pl.ds(8 * tp, 8), 0:B]
     load_fg.wait()
     load_fb.wait()
+    fgain = upright(fgain_v[...])
+    fbias = upright(fbias_v[...])
 
     sent(plane, NX * NTP - 1, 0)
     sent(wq_v, NX - 1, 1)
@@ -387,7 +401,7 @@
     sent(down_buf, NTP - 1, 14)
     sent(ost, NKV - 1, 15)
     mean, rstd = stats(ost, 15)
-    result = (outer - to_col(mean)) * to_col(rstd) * fgain_v[...] + fbias_v[...]
+    result = (outer - mean[:, 0:B]) * rstd[:, 0:B] * fgain + fbias
     out[...] = result.astype(BF16)
 
 
@@ -397,21 +411,21 @@
 ):
     vmem = pltpu.VMEM
     scratch = [
-        vmem((B, 8), BF16),
+        vmem((8, B), BF16),
         vmem((1, 8), F32),
         vmem((1, 8), F32),
         vmem((1, 8), F32),
         vmem((1, 8), F32),
         vmem((NX, 64, 128), BF16),
         vmem((NX, 2, 64, 128), BF16),
-        vmem((NX * 64, 8), BF16),
-        vmem((128, 64), BF16),
+        vmem((8, NX * 64), BF16),
+        vmem((64, 128), BF16),
         vmem((64, 1024), BF16),
-        vmem((1024, 64), BF16),
+        vmem((64, 1024), BF16),
         vmem((B, POS, 128), BF16),
         vmem((B, POS, 128), BF16),
         vmem((B, 1, POS), F32),
-        vmem((128, 128), F32),
+        vmem((8, 128), F32),
         vmem((NX * NTP, 8, 128), F32),
         vmem((NZ, B, 128), F32),
         vmem((NZ, 2, 384), F32),
@@ -430,31 +444,32 @@
         vmem((B, 2, 4, 128), F32),
         vmem((NTP, 8, 128), F32),
         vmem((NKV, 1, 128), F32),
+        vmem((128, 128), F32),
         pltpu.SemaphoreType.DMA((13,)),
         pltpu.SemaphoreType.DMA((4,)),
         pltpu.SemaphoreType.DMA((4,)),
         pltpu.SemaphoreType.DMA((16,)),
         pltpu.SemaphoreType.DMA((16,)),
     ]
-    any_space = pl.BlockSpec(memory_space=pl.ANY)
+    any_space = pl.BlockSpec(memory_space=pltpu.HBM)
     return pl.pallas_call(
         body,
-        out_shape=jax.ShapeDtypeStruct((B, 8), BF16),
+        out_shape=jax.ShapeDtypeStruct((8, B), BF16),
         in_specs=[any_space] * 15,
         out_specs=pl.BlockSpec(memory_space=pltpu.VMEM),
         scratch_shapes=scratch,
         compiler_params=pltpu.CompilerParams(
-            collective_id=0, has_side_effects=True, vmem_limit_bytes=48 * 1024 * 1024
+            collective_id=0, has_side_effects=True, vmem_limit_bytes=67043328
         ),
         name="step",
     )(
-        tokens, w_query, w_key, w_value, w_forget, w_out,
+        tokens.T, w_query, w_key, w_value, w_forget.T, w_out.T,
         mix_gain.reshape(1, 8), mix_bias.reshape(1, 8),
         ffn_gain.reshape(1, 8), ffn_bias.reshape(1, 8),
-        w_up, down_weight,
+        w_up, down_weight.T,
         cache_keys.reshape(B, POS, HEAD_DIM), cache_values.reshape(B, POS, HEAD_DIM),
         cum_gates,
-    )
+    ).T
 
 
 def solution(mesh):

time: 72.2 us -> 59.7 us (0.83)
  local copies, waits for them, and re-layouts: 14 us -> 1.26 us
    unnamed x26 -> x1, local copies, waits for them, and re-layouts: 13.3 us -> 1.26 us
where the time goes in v2:
time: 59.7 us; the launch traced here: 59.6 us
  Pallas kernels  58.3 us (98%)
  local copies, waits for them, and re-layouts  1.26 us (2%)
    pallas_call x1, Pallas kernels, shards(): pl.pallas_call(body, out_shape=jax.ShapeDtypeStruct((8, B), BF16), in_spe...  58.3 us
    unnamed x1, local copies, waits for them, and re-layouts  1.26 us

profile of v2, /device:TPU:1, one launch (start us, length us, event | category | flops | bytes accessed | tf_op | source)
XLA Modules:
  0.0 59.6 jit_solution(11724742812080183211)
XLA Ops:
  0.0 58.3 %step.1 = bf16[8,16]{1,0:T(8,128)(2,1)} custom-call(bf16[8,16]{1,0:T(8,128)(2,1)} %bitcast.17, bf16[64,128]{1,0:T(8,128)(2,1)} %w_query.1, bf16[64,128]{1,0:T(8,128)(2,1)} %w_key.1, bf16[64,128]{1,0:T(8,128)(2,1)} %w_value.1, bf16[8,2048]{1,0:T(8,128)(2,1)} %bitcast.14, bf16[64,128]{1,0:T(8,128)(2,1)} %bitcast.15, f32[1,8]{1,0:T(1,128)} %bitcast.18, ...), custom_call_target="tpu_custom_call" | custom-call | tf_op jit(solution)/shard_map/step/pallas_call | solution.py:455
  58.4 1.3 %copy.17 = bf16[16,8]{0,1:T(8,128)(2,1)} copy(bf16[16,8]{0,1:T(8,128)(2,1)} %bitcast.16) | data formatting | bytes 512

commit v3 on v2

--- a/solution.py
+++ b/solution.py
@@ -29,7 +29,7 @@
     w_up, w_down, keys, values, gates,
     out,
     tok_v, gain_v, bias_v, fgain_v, fbias_v, wq_v, wkv_v, wf_v, wo_v, wup_v, wdn_v, k_v, v_v, cg_v,
-    stage, plane, q_buf, kvg_send, kvg_buf, gwb_send, gwb_buf, accx, stx, accz, stz, head_buf,
+    gb_buf, plane, q_buf, kvg_send, kvg_buf, gwb_send, gwb_buf, accx, stx, accz, stz, head_buf,
     mst, up_send, up_buf, hid_buf, hid_f, down_buf, ost, turned,
     load_sem, k_sem, v_sem, send_sem, recv_sem,
 ):
@@ -40,26 +40,27 @@
 
     barrier = pltpu.get_barrier_semaphore()
 
-    def plane_peer(i):
-        t = i // NTP
-        r = i % NTP
-        px = (x + NX - 1 - t + NX) % NX
-        py = (y + NY - 1 - r // NC + NY) % NY
-        pc = (c + NC - 1 - r % NC) % NC
-        return {"x": px, "y": py, "c": pc}
-
-    def greet_plane(i, carry):
-        pl.semaphore_signal(barrier, inc=1, device_id=plane_peer(i), device_id_type=MESH)
-        return carry
-
-    def greet_line(i, carry):
-        pl.semaphore_signal(
-            barrier, inc=1, device_id={"z": (z + 1 + i) % NZ}, device_id_type=MESH
-        )
-        return carry
-
-    lax.fori_loop(0, NZ - 1, greet_line, 0)
-    lax.fori_loop(0, NX * NTP - 1, greet_plane, 0)
+    xs = [x] + [lax.rem(x + i, NX) for i in range(1, NX)]
+    ys = [y] + [lax.rem(y + i, NY) for i in range(1, NY)]
+    cs = [c, 1 - c]
+    zs = [z] + [lax.rem(z + i, NZ) for i in range(1, NZ)]
+    line = (4, 3, 5, 2, 6, 1, 7)
+    ring = (2, 1, 3)
+    x_peers = [{"x": xs[i]} for i in ring]
+    z_peers = [{"z": zs[i]} for i in line]
+    tp_peers = [{"y": ys[i], "c": cs[j]} for i in ring for j in (1, 0)] + [{"c": cs[1]}]
+    offsets = [(i, j, k) for i in (0, 2, 1, 3) for j in (0, 2, 1, 3) for k in (1, 0)]
+    far = {0: 0, 1: 1, 2: 2, 3: 1}
+    offsets = sorted(offsets, key=lambda o: -(far[o[0]] + far[o[1]]))[:-2] + [(0, 0, 1)]
+    plane_peers = [{"x": xs[i], "y": ys[j], "c": cs[k]} for i, j, k in offsets]
+    pairs = sorted(
+        [(i, j) for i in range(NZ) for j in range(NX) if i or j],
+        key=lambda o: -(min(o[0], NZ - o[0]) + far[o[1]]),
+    )
+    kv_peers = [{"z": zs[i], "x": xs[j]} for i, j in pairs]
+
+    for peer in z_peers + plane_peers:
+        pl.semaphore_signal(barrier, inc=1, device_id=peer, device_id_type=MESH)
 
     loads = []
 
@@ -77,14 +78,14 @@
     load_k = load(w_key, wkv_v.at[x, 0], load_sem.at[4])
     load_v = load(w_value, wkv_v.at[x, 1], load_sem.at[5])
     load_f = load(w_forget.at[:, pl.ds(z * NX * 64, NX * 64)], wf_v, load_sem.at[6])
-    load_o = load(w_out, wo_v, load_sem.at[7])
+    load_o = [load(w_out, wo_v.at[pl.ds(64 * i, 64)], load_sem.at[7 + 6 * i]) for i in range(2)]
     load_up = load(w_up, wup_v, load_sem.at[8])
     load_fg = load(ffn_gain, fgain_v, load_sem.at[9])
     load_fb = load(ffn_bias, fbias_v, load_sem.at[10])
     load_cg = load(gates, cg_v, load_sem.at[11])
     load_key = [load(keys.at[pl.ds(4 * i, 4)], k_v.at[pl.ds(4 * i, 4)], k_sem.at[i]) for i in range(4)]
     load_val = [load(values.at[pl.ds(4 * i, 4)], v_v.at[pl.ds(4 * i, 4)], v_sem.at[i]) for i in range(4)]
-    load_dn = load(w_down, wdn_v, load_sem.at[12])
+    load_dn = [load(w_down, wdn_v.at[pl.ds(64 * i, 64)], load_sem.at[12 + 2 * i]) for i in range(2)]
 
     lane = lax.broadcasted_iota(jnp.int32, (B, 128), 1)
     row = lax.broadcasted_iota(jnp.int32, (B, 128), 0)
@@ -102,6 +103,7 @@
 
     for copy in first:
         copy.wait()
+    plane[slot, :, 0:B] = tok_v[...]
     lane_8 = lax.broadcasted_iota(jnp.int32, (8, 128), 1)
     diag_8 = lax.broadcasted_iota(jnp.int32, (8, 8), 0) == lax.broadcasted_iota(
         jnp.int32, (8, 8), 1
@@ -112,11 +114,9 @@
             jnp.where(diag_8, jnp.broadcast_to(line, (8, 8)), 0.0), axis=1, keepdims=True
         )
 
-    stage[...] = jnp.where(
-        lane_8 == B, upright(gain_v[...]), jnp.where(lane_8 == B + 1, upright(bias_v[...]), 0.0)
-    )
-    stage[:, 0:B] = tok_v[...].astype(F32)
-    plane[slot] = stage[...]
+    gb_buf[tp] = jnp.where(
+        lane_8 == 0, upright(gain_v[...]), jnp.where(lane_8 == 1, upright(bias_v[...]), 0.0)
+    )
     load_q.wait()
     load_k.wait()
     load_v.wait()
@@ -141,34 +141,21 @@
         part = ref.at[pl.ds(0, count)]
         pltpu.make_async_copy(part, part, send_sem.at[phase]).wait()
 
-    def line_peer(i):
-        step = (i + 1) // 2 * (2 * (i % 2) - 1) + 4
-        return (z + step + NZ) % NZ
-
-    def kv_peer(i):
-        t = i // NX
-        step = (t + 1) // 2 * (2 * (t % 2) - 1) + 4
-        return (z + step + NZ) % NZ, (x + NX - 1 - i % NX) % NX
-
-    def loop(count, f):
-        def step(i, carry):
-            f(i)
-            return carry
-
-        lax.fori_loop(0, count, step, 0)
-
-    loop(NX * NTP - 1, lambda i: push(plane.at[slot], plane.at[slot], 0, plane_peer(i)))
-    loop(NX - 1, lambda i: push(wq_v.at[x], wq_v.at[x], 1, {"x": (x + NX - 1 - i) % NX}))
-    loop(NX - 1, lambda i: push(wkv_v.at[x], wkv_v.at[x], 2, {"x": (x + NX - 1 - i) % NX}))
+    def spread_out(ref, phase, peers):
+        for peer in peers:
+            push(ref, ref, phase, peer)
+
+    spread_out(plane.at[slot], 0, plane_peers)
+    spread_out(wq_v.at[x], 1, x_peers)
+    spread_out(wkv_v.at[x], 2, x_peers)
+    spread_out(gb_buf.at[tp], 16, tp_peers)
 
     received(plane, NX * NTP - 1, 0)
-    spread = plane[...].reshape(NX * NTP * 8, 128).T
+    spread = plane[...].astype(F32).reshape(NX * NTP * 8, 128).T
     tok = spread[0:B, :].astype(BF16)
     received(wq_v, NX - 1, 1)
     q_buf[z] = jnp.dot(tok, wq_v[...].reshape(NX * 64, HEAD_DIM), preferred_element_type=F32)
-    loop(
-        NZ - 1, lambda i: push(q_buf.at[z], q_buf.at[z], 3, {"z": line_peer(i)})
-    )
+    spread_out(q_buf.at[z], 3, z_peers)
     received(wkv_v, NX - 1, 2)
     load_f.wait()
     key_part = jnp.dot(tok, wkv_v[:, 0].reshape(NX * 64, HEAD_DIM), preferred_element_type=F32)
@@ -182,21 +169,20 @@
         kvg_send[i, :, 128:256] = value_part[2 * i : 2 * i + 2, :]
         kvg_send[i, :, 256:384] = gate_part[2 * i : 2 * i + 2, :]
     kvg_buf[z] = kvg_send[z]
-
-    def push_kvg(i):
-        pz = line_peer(i)
-        push(kvg_send.at[pz], kvg_buf.at[z], 4, {"z": pz})
-
-    loop(NZ - 1, push_kvg)
-
-    own = jnp.where(x >= 2, spread[0:24, 128:256], spread[0:24, 0:128])
-    own = jnp.where(x % 2 == 1, pltpu.roll(own, 64, 1), own)
-    tok_own = own[0:B, :]
-    gain_own = own[B : B + 1, :]
-    bias_own = own[B + 1 : B + 2, :]
+    for peer in z_peers:
+        push(kvg_send.at[peer["z"]], kvg_buf.at[z], 4, peer)
+
+    own = jnp.where(x >= 2, spread[0:B, 128:256], spread[0:B, 0:128])
+    tok_own = jnp.where(x % 2 == 1, pltpu.roll(own, 64, 1), own)
+    received(gb_buf, NTP - 1, 16)
+    both = jnp.concatenate(
+        [gb_buf[...].reshape(64, 128), jnp.zeros((64, 128), F32)], axis=0
+    ).T
+    gain_own = both[0:1, :]
+    bias_own = both[1:2, :]
 
     load_up.wait()
-    both = jnp.concatenate([gain_own, bias_own], axis=0)[:, 0:64]
+    both = both[0:2, 0:64]
     both_hi = both.astype(BF16)
     both_lo = (both - both_hi.astype(F32)).astype(BF16)
     gwb = jnp.dot(
@@ -212,14 +198,11 @@
             gwb_send[h, 4 + j : 5 + j, :] = gwb[1:2, at : at + 128]
     gwb_buf[kv] = gwb_send[kv % 2]
 
+    for peer in kv_peers:
+        push(gwb_send.at[lax.rem(peer["x"], 2)], gwb_buf.at[kv], 5, peer)
+
     received(q_buf, NZ - 1, 3)
     query = jnp.sum(q_buf[...], axis=0).astype(BF16)
-
-    def push_gwb(i):
-        pz, px = kv_peer(i)
-        push(gwb_send.at[px % 2], gwb_buf.at[kv], 5, {"z": pz, "x": px})
-
-    loop(NKV - 1, push_gwb)
 
     load_cg.wait()
     row_pos = lax.broadcasted_iota(jnp.int32, (B, POS), 0)
@@ -260,9 +243,9 @@
     acc = acc + own_weight * value_new
 
     stx[x] = jnp.concatenate([to_row(peak, diag), to_row(total, diag)], axis=0)
-    loop(NX - 1, lambda i: push(stx.at[x], stx.at[x], 7, {"x": (x + NX - 1 - i) % NX}))
+    spread_out(stx.at[x], 7, x_peers)
     accx[x] = acc
-    loop(NX - 1, lambda i: push(accx.at[x], accx.at[x], 6, {"x": (x + NX - 1 - i) % NX}))
+    spread_out(accx.at[x], 6, x_peers)
 
     def combine(acc_ref, st_ref, count, acc_phase, st_phase):
         received(st_ref, count - 1, st_phase)
@@ -281,44 +264,33 @@
             acc = acc + cols[i] * acc_ref[i]
         return peak, total, acc
 
-    load_o.wait()
-    w_out2 = jnp.concatenate([wo_v[...], wo_v[...]], axis=0)
-    load_dn.wait()
-    w_down2 = jnp.concatenate([wdn_v[...], wdn_v[...]], axis=0)
-
+    for copy in load_o + load_dn:
+        copy.wait()
     peak, total, acc = combine(accx, stx, NX, 6, 7)
     stz[z] = jnp.concatenate([peak, total], axis=0)
-    loop(NZ - 1, lambda i: push(stz.at[z], stz.at[z], 9, {"z": line_peer(i)}))
+    spread_out(stz.at[z], 9, z_peers)
     accz[z] = acc
-    loop(NZ - 1, lambda i: push(accz.at[z], accz.at[z], 8, {"z": line_peer(i)}))
+    spread_out(accz.at[z], 8, z_peers)
     peak, total, acc = combine(accz, stz, NZ, 8, 9)
     attended = (acc / to_col(total)).astype(BF16)
 
     lane_half = lax.broadcasted_iota(jnp.int32, (8, 128), 1) < 64
 
-    def tp_peer(i):
-        return {"y": (y + NY - 1 - i // NC) % NY, "c": (c + NC - 1 - i % NC) % NC}
-
     def tp_sum(terms, ref, phase):
         ref[tp] = jnp.where(lane_half, terms[0:8, :], terms[8:16, :])
-        loop(NTP - 1, lambda i: push(ref.at[tp], ref.at[tp], phase, tp_peer(i)))
+        spread_out(ref.at[tp], phase, tp_peers)
         received(ref, NTP - 1, phase)
         summed = jnp.sum(ref[...], axis=0)
         return jnp.concatenate([summed, pltpu.roll(summed, 64, 1)], axis=0)
 
-    head_terms = tp_sum(across(attended, w_out2), head_buf, 10)
+    head_terms = tp_sum(across(attended, wo_v[...]), head_buf, 10)
     mixed = jnp.where(lane < 64, ROOT2 * tok_own + head_terms, 0.0)
 
     def push_stats(values, ref, phase):
         sums = jnp.sum(values, axis=1, keepdims=True)
         squares = jnp.sum(values * values, axis=1, keepdims=True)
         ref[kv] = to_row(sums, diag) + to_row(squares, diag16)
-
-        def push_one(i):
-            pz, px = kv_peer(i)
-            push(ref.at[kv], ref.at[kv], phase, {"z": pz, "x": px})
-
-        loop(NKV - 1, push_one)
+        spread_out(ref.at[kv], phase, kv_peers)
 
     def stats(ref, phase):
         received(ref, NKV - 1, phase)
@@ -344,11 +316,9 @@
             up_send[:, h, j, :] = up[:, at : at + 128]
     up_buf[kv] = up_send[kv // 2, kv % 2]
 
-    def push_up(i):
-        pz, px = kv_peer(i)
-        push(up_send.at[2 * pz + px // 2, px % 2], up_buf.at[kv], 12, {"z": pz, "x": px})
-
-    loop(NKV - 1, push_up)
+    for peer in kv_peers:
+        px = peer["x"]
+        push(up_send.at[2 * peer["z"] + px // 2, lax.rem(px, 2)], up_buf.at[kv], 12, peer)
     received(gwb_buf, NKV - 1, 5)
     gwb = jnp.sum(gwb_buf[...], axis=0)
     mean, rstd = stats(mst, 11)
@@ -360,12 +330,7 @@
     up_row = rstd_here * (up_sum - mean_here * gwb[0:4, :]) + gwb[4:8, :]
     hidden = jnp.square(jnp.maximum(up_row, 0.0)).astype(BF16)
     hid_buf[kv] = hidden
-
-    def push_hidden(i):
-        pz, px = kv_peer(i)
-        push(hid_buf.at[kv], hid_buf.at[kv], 13, {"z": pz, "x": px})
-
-    loop(NKV - 1, push_hidden)
+    spread_out(hid_buf.at[kv], 13, kv_peers)
 
     normed = (mixed - to_col(mean)) * to_col(rstd) * gain_own + bias_own
     normed = normed.astype(BF16).astype(F32)
@@ -374,7 +339,7 @@
     hidden_all = jnp.concatenate(
         [hid_f[:, h, j, :].astype(BF16) for h in range(2) for j in range(4)], axis=1
     )
-    down_terms = tp_sum(across(hidden_all, w_down2), down_buf, 14)
+    down_terms = tp_sum(across(hidden_all, wdn_v[...]), down_buf, 14)
     outer = jnp.where(lane < 64, ROOT2 * normed + down_terms, 0.0)
     push_stats(outer, ost, 15)
     turned[...] = jnp.concatenate([outer, jnp.zeros((128 - B, 128), F32)], axis=0).T
@@ -400,6 +365,7 @@
     sent(hid_buf, NKV - 1, 13)
     sent(down_buf, NTP - 1, 14)
     sent(ost, NKV - 1, 15)
+    sent(gb_buf, NTP - 1, 16)
     mean, rstd = stats(ost, 15)
     result = (outer - mean[:, 0:B]) * rstd[:, 0:B] * fgain + fbias
     out[...] = result.astype(BF16)
@@ -419,14 +385,14 @@
         vmem((NX, 64, 128), BF16),
         vmem((NX, 2, 64, 128), BF16),
         vmem((8, NX * 64), BF16),
-        vmem((64, 128), BF16),
+        vmem((128, 128), BF16),
         vmem((64, 1024), BF16),
-        vmem((64, 1024), BF16),
+        vmem((128, 1024), BF16),
         vmem((B, POS, 128), BF16),
         vmem((B, POS, 128), BF16),
         vmem((B, 1, POS), F32),
-        vmem((8, 128), F32),
-        vmem((NX * NTP, 8, 128), F32),
+        vmem((NTP, 8, 128), F32),
+        vmem((NX * NTP, 8, 128), BF16),
         vmem((NZ, B, 128), F32),
         vmem((NZ, 2, 384), F32),
         vmem((NZ, 2, 384), F32),
@@ -445,11 +411,11 @@
         vmem((NTP, 8, 128), F32),
         vmem((NKV, 1, 128), F32),
         vmem((128, 128), F32),
-        pltpu.SemaphoreType.DMA((13,)),
+        pltpu.SemaphoreType.DMA((15,)),
         pltpu.SemaphoreType.DMA((4,)),
         pltpu.SemaphoreType.DMA((4,)),
-        pltpu.SemaphoreType.DMA((16,)),
-        pltpu.SemaphoreType.DMA((16,)),
+        pltpu.SemaphoreType.DMA((17,)),
+        pltpu.SemaphoreType.DMA((17,)),
     ]
     any_space = pl.BlockSpec(memory_space=pltpu.HBM)
     return pl.pallas_call(

time: 59.7 us -> 57.5 us (0.963)
  Pallas kernels: 58.3 us -> 56.1 us
    pallas_call x1, Pallas kernels: 58.3 us -> 56.1 us  [shards(): pl.pallas_call(body, out_shape=jax.ShapeDtypeStruct((8, B), BF16), in_spe...]
where the time goes in v3:
time: 57.5 us; the launch traced here: 57.4 us
  Pallas kernels  56.1 us (98%)
  local copies, waits for them, and re-layouts  1.26 us (2%)
    pallas_call x1, Pallas kernels, shards(): pl.pallas_call(body, out_shape=jax.ShapeDtypeStruct((8, B), BF16), in_spe...  56.1 us
    unnamed x1, local copies, waits for them, and re-layouts  1.26 us

profile of v3, /device:TPU:1, one launch (start us, length us, event | category | flops | bytes accessed | tf_op | source)
XLA Modules:
  0.0 57.4 jit_solution(17294294499853292354)
XLA Ops:
  0.0 56.1 %step.1 = bf16[8,16]{1,0:T(8,128)(2,1)} custom-call(bf16[8,16]{1,0:T(8,128)(2,1)} %bitcast.17, bf16[64,128]{1,0:T(8,128)(2,1)} %w_query.1, bf16[64,128]{1,0:T(8,128)(2,1)} %w_key.1, bf16[64,128]{1,0:T(8,128)(2,1)} %w_value.1, bf16[8,2048]{1,0:T(8,128)(2,1)} %bitcast.14, bf16[64,128]{1,0:T(8,128)(2,1)} %bitcast.15, f32[1,8]{1,0:T(1,128)} %bitcast.18, ...), custom_call_target="tpu_custom_call" | custom-call | tf_op jit(solution)/shard_map/step/pallas_call | solution.py:421
  56.1 1.3 %copy.17 = bf16[16,8]{0,1:T(8,128)(2,1)} copy(bf16[16,8]{0,1:T(8,128)(2,1)} %bitcast.16) | data formatting | bytes 512
